TPU v7x, 32 devices: a whole 2x2x4 slice. The times are simulated.
32 devices in a mesh: sp: 16 (over z, y, x), tp: 2 (over core).
Axes of the slice: x: 2, y: 2, z: 4, core: 2. Of those that a mesh axis runs over, the one named last changes fastest.
Arguments:
- stream: bfloat16 [6144, 2048], P('sp'), may hold values from -40 to 40
- query_rows: bfloat16 [6144, 1024], P('sp', 'tp'), may hold values from -10 to 10
- key_rows: bfloat16 [6144, 256], P('sp'), may hold values from -10 to 10
- value_rows: bfloat16 [6144, 256], P('sp'), may hold values from -6 to 6
- doc_ids: int32 [6144], P('sp'), may hold values from 0 to 7, never falling along the last dimension, each value on 1 to 1536 neighbouring positions
- sink_logit: float32 [8], P('tp'), may hold values from 2 to 7
- out_weight: bfloat16 [1024, 2048], P('tp'), may hold values from -1.5 to 1.5
- norm_gain: float32 [2048], replicated, may hold values from 0.1 to 1.9
- gate_weight: bfloat16 [2048, 5632], P('sp', 'tp'), may hold values from -0.125 to 0.125
- up_weight: bfloat16 [2048, 5632], P('sp', 'tp'), may hold values from -0.125 to 0.125
- down_weight: bfloat16 [5632, 2048], P('tp', 'sp'), may hold values from -0.078125 to 0.078125
Outputs:
- mixed_out: bfloat16 [6144, 2048], P('sp')
Inputs may be any that keep to these rules, and one draw needn't show every extreme that they name: `doc_ids`: document numbers never fall along the sequence; each document has 1 to 1536 positions.
All inputs are finite; a program needn't handle non-finite values.
Results may differ from a plain program's by a relative error of at most 0.009.
Values may be sent and summed in bfloat16 or wider, within the bound.
No kernel may reach another device: no remote copies, remote signals or barrier semaphores. Data moves between devices by JAX's collectives and lax.ppermute only.
A program may use at most 128 MiB of HBM per device.

v0:
```python
import jax
import jax.numpy as jnp
from jax import lax
from jax.sharding import PartitionSpec as P

HEADS = 8
KVH = 2
HD = 128
WIN = 128
norm_eps = 1e-06
masked_low = -1e30


def extended(value, sides, width):
    for axis, dim in sides:
        peers, length = (lax.axis_size(axis), value.shape[dim])
        up = [(i, (i + 1) % peers) for i in range(peers - 1)]
        down = [(j, i) for i, j in up]
        last = lax.slice_in_dim(value, length - width, length, axis=dim)
        initial = lax.slice_in_dim(value, 0, width, axis=dim)
        before = lax.ppermute(last, axis, up)
        after = lax.ppermute(initial, axis, down)
        value = jnp.concatenate([before, value, after], axis=dim)
    return value


def per_device(
    stream,
    query_rows,
    key_rows,
    value_rows,
    doc_ids,
    sink_logit,
    out_weight,
    norm_gain,
    gate_weight,
    up_weight,
    down_weight,
):
    row_count = stream.shape[0]
    heads_here = query_rows.shape[1] // HD
    group_share = HEADS // KVH
    groups_here = max(1, heads_here // group_share)
    per_group = heads_here // groups_here
    tp_place = lax.axis_index("tp")
    group_first = tp_place * heads_here // group_share
    keys_here = lax.dynamic_slice_in_dim(key_rows, group_first * HD, groups_here * HD, 1)
    values_here = lax.dynamic_slice_in_dim(value_rows, group_first * HD, groups_here * HD, 1)
    keys_wide, values_wide, docs_wide = (
        extended(keys_here, (("sp", 0),), WIN),
        extended(values_here, (("sp", 0),), WIN),
        extended(doc_ids, (("sp", 0),), WIN),
    )
    seq_offset = lax.axis_index("sp") * row_count
    seq_total = row_count * lax.axis_size("sp")
    query_pos = seq_offset + jnp.arange(row_count, dtype=jnp.int32)
    key_pos = seq_offset - WIN + jnp.arange(row_count + 2 * WIN, dtype=jnp.int32)
    allowed = (
        (jnp.abs(query_pos[:, None] - key_pos[None, :]) <= WIN)
        & (key_pos[None, :] >= 0)
        & (key_pos[None, :] < seq_total)
        & (doc_ids[:, None] == docs_wide[None, :])
    )
    queries = query_rows.reshape(row_count, groups_here, per_group, HD)
    keys_grid = keys_wide.reshape(row_count + 2 * WIN, groups_here, HD)
    values_grid = values_wide.reshape(row_count + 2 * WIN, groups_here, HD)
    scores = jnp.einsum(
        "qgrd,kgd->grqk", queries, keys_grid, preferred_element_type=jnp.float32
    ) * HD ** (-0.5)
    masked = jnp.where(allowed[None, None], scores, masked_low)
    sinks = sink_logit.reshape(groups_here, per_group, 1, 1)
    peak = jnp.maximum(jnp.max(masked, axis=-1, keepdims=True), sinks)
    lifted = jnp.where(allowed[None, None], jnp.exp(masked - peak), 0.0)
    denom = jnp.sum(lifted, axis=-1, keepdims=True) + jnp.exp(sinks - peak)
    probs = (lifted / denom).astype(jnp.bfloat16)
    attended = jnp.einsum("grqk,kgd->qgrd", probs, values_grid, preferred_element_type=jnp.float32)
    attended = attended.astype(jnp.bfloat16).reshape(row_count, heads_here * HD)
    partial_value = jnp.dot(attended, out_weight, preferred_element_type=jnp.float32)
    branch = lax.psum(partial_value.astype(jnp.bfloat16), "tp")
    carried = (stream.astype(jnp.float32) + branch.astype(jnp.float32)).astype(jnp.bfloat16)
    carried_f = carried.astype(jnp.float32)
    normed = (
        carried_f
        * lax.rsqrt(jnp.mean(carried_f * carried_f, axis=1, keepdims=True) + norm_eps)
        * norm_gain[None, :]
    ).astype(jnp.bfloat16)

    def add_rows(weight_rows):
        return jnp.dot(normed, weight_rows, preferred_element_type=jnp.float32)

    gate_acc = add_rows(lax.all_gather(gate_weight, "sp", axis=0, tiled=True))
    up_acc = add_rows(lax.all_gather(up_weight, "sp", axis=0, tiled=True))
    hidden = (jax.nn.silu(gate_acc) * up_acc).astype(jnp.bfloat16)
    terms = jnp.dot(
        hidden,
        lax.all_gather(down_weight, "sp", axis=1, tiled=True),
        preferred_element_type=jnp.float32,
    )
    feed = lax.psum(terms.astype(jnp.bfloat16), "tp")
    return (carried_f + 0.5 * feed.astype(jnp.float32)).astype(jnp.bfloat16)


def solution(mesh):
    in_specs = (
        P("sp", None),
        P("sp", "tp"),
        P("sp", None),
        P("sp", None),
        P("sp"),
        P("tp"),
        P("tp", None),
        P(),
        P("sp", "tp"),
        P("sp", "tp"),
        P("tp", "sp"),
    )
    out_specs = P("sp", None)
    return jax.shard_map(
        per_device, mesh=mesh, in_specs=in_specs, out_specs=out_specs, check_vma=False
    )
```

profile of v0, /device:TPU:0, one launch (start us, length us, event | category | flops | bytes accessed | tf_op | source)
XLA Modules:
  0.0 561.7 jit_solution(12022949672108720570)
XLA Ops:
  7.4 0.9 fusion.38
  8.3 4.9 collective-permute-start.4
  13.2 1.3 collective-permute-start.5
  14.5 0.8 fusion.40
  15.2 4.5 collective-permute-start.2
  19.8 1.3 collective-permute-start.3
  21.1 1.0 constant_dynamic-slice_fusion.1
  22.2 4.9 collective-permute-start
  27.2 1.3 collective-permute-start.1
  28.5 0.7 pad_add_fusion
  29.2 1.4 fusion.14
  30.6 1.8 fusion.1
  32.5 1.0 fusion.6
  33.9 1.5 fusion.9
  35.4 2.2 convolution_convert_fusion.1
  39.6 23.8 %all-reduce.3.cloned.1.call-done = bf16[384,2048]{1,0:T(8,128)(2,1)} async-done(((bf16[384,2048]{1,0:T(8,128)(2,1)}), bf16[384,2048]{1,0:T(8,128)(2,1)}) %all-reduce.3.cloned.1.call-update) | async-done | bytes 1572880 | tf_op jit(solution)/shard_map/psum | solution.py:79
  63.3 3.6 fusion.2
  66.9 120.3 %all-gather.4.cloned.1.call-done = bf16[2048,2816]{1,0:T(8,128)(2,1)} async-done(((bf16[128,2816]{1,0:T(8,128)(2,1)}), bf16[2048,2816]{1,0:T(8,128)(2,1)}) %all-gather.4.cloned.1.call-update) | async-done | bytes 11534352 | tf_op jit(solution)/shard_map/all_gather | solution.py:91
  187.2 11.5 %fusion.17 = f32[384,2816]{1,0:T(8,128)} fusion(bf16[2048,2816]{1,0:T(8,128)(2,1)} %all-gather.4.cloned.1.call-done, bf16[384,2048]{1,0:T(8,128)(2,1)} %get-tuple-element.6, f32[2048]{0:T(1024)S(1)} %copy-done.2, f32[384]{0:T(512)S(1)} %add_rsqrt_fusion), kind=kOutput, calls=%fused_computation.24 | convolution fusion | flops 4432330752 | bytes 17442304 | tf_op jit(solution)/shard_map/dot_general | solution.py:89
  198.8 130.5 %all-gather.6.cloned.1.call-done = bf16[2048,2816]{1,0:T(8,128)(2,1)} async-done(((bf16[128,2816]{1,0:T(8,128)(2,1)}), bf16[2048,2816]{1,0:T(8,128)(2,1)}) %all-gather.6.cloned.1.call-update) | async-done | bytes 11534352 | tf_op jit(solution)/shard_map/all_gather | solution.py:92
  329.3 182.7 %all-gather.8.cloned.1.call-done = bf16[2816,2048]{1,0:T(8,128)(2,1)} async-done(((bf16[2816,128]{1,0:T(8,128)(2,1)}), bf16[2816,2048]{1,0:T(8,128)(2,1)}) %all-gather.8.cloned.1.call-update) | async-done | bytes 11534352 | tf_op jit(solution)/shard_map/all_gather | solution.py:96
  511.9 19.8 %convolution_convert_fusion = bf16[384,2048]{1,0:T(8,128)(2,1)} fusion(bf16[2816,2048]{1,0:T(8,128)(2,1)} %all-gather.8.cloned.1.call-done, bf16[2048,2816]{1,0:T(8,128)(2,1)} %all-gather.6.cloned.1.call-done, f32[384,2816]{1,0:T(8,128)} %fusion.17, bf16[384,2048]{1,0:T(8,128)(2,1)} %get-tuple-element.6, f32[2048]{0:T(1024)S(1)} %copy-done.2, ...), kind=kOutput, calls=%fused_computation.14 | convolution fusion | flops 8868790272 | bytes 30549504 | tf_op jit(solution)/shard_map/dot_general | solution.py:94
  531.7 18.7 %all-reduce.5.cloned.1.call-done = bf16[384,2048]{1,0:T(8,128)(2,1)} async-done(((bf16[384,2048]{1,0:T(8,128)(2,1)}), bf16[384,2048]{1,0:T(8,128)(2,1)}) %all-reduce.5.cloned.1.call-update) | async-done | bytes 1572880 | tf_op jit(solution)/shard_map/psum | solution.py:99
  550.5 3.7 fusion.5
  (30 shorter events, 2.6 us)
Async XLA Ops:
  7.4 28.0 %copy-start = (bf16[512,2048]{1,0:T(8,128)(2,1)S(1)}, bf16[512,2048]{1,0:T(8,128)(2,1)}, u32[]{:S(2)}) copy-start(bf16[512,2048]{1,0:T(8,128)(2,1)} %param.17) | copy-start | bytes 6291460
  7.4 25.1 %copy-start.1 = (f32[4]{0:T(128)S(1)}, f32[4]{0:T(128)}, u32[]{:S(2)}) copy-start(f32[4]{0:T(128)} %param.16) | copy-start | bytes 52
  7.4 56.0 %all-reduce.3.cloned.1.call-start = ((), (), s32[]{:S(2)}) async-start(), calls=%async_computation | async-start | bytes 3145728 | tf_op jit(solution)/shard_map/psum | solution.py:79
  8.3 22.3 %collective-permute-start.4 = (bf16[128,128]{1,0:T(8,128)(2,1)S(1)}, bf16[128,128]{1,0:T(8,128)(2,1)S(1)}, u32[]{:S(2)}, u32[]{:S(2)}) collective-permute-start(bf16[128,128]{1,0:T(8,128)(2,1)S(1)} %get-tuple-element.7), channel_id=1, source_target_pairs={{0,2},{2,4},{4,6},{6,8},{8,10},{10,12},{12,14},{14,16},{16,18},{18... | collective-permute-start | bytes 98312 | tf_op jit(solution)/shard_map/ppermute | solution.py:21
  13.2 17.4 %collective-permute-start.5 = (bf16[128,128]{1,0:T(8,128)(2,1)S(1)}, bf16[128,128]{1,0:T(8,128)(2,1)S(1)}, u32[]{:S(2)}, u32[]{:S(2)}) collective-permute-start(bf16[128,128]{1,0:T(8,128)(2,1)S(1)} %get-tuple-element.8), channel_id=1, source_target_pairs={{2,0},{4,2},{6,4},{8,6},{10,8},{12,10},{14,12},{16,14},{18,16},{20... | collective-permute-start | bytes 98312 | tf_op jit(solution)/shard_map/ppermute | solution.py:22
  15.2 11.9 %collective-permute-start.2 = (s32[128]{0:T(128)S(1)}, s32[128]{0:T(128)S(1)}, u32[]{:S(2)}, u32[]{:S(2)}) collective-permute-start(s32[128]{0:T(128)S(1)} %get-tuple-element.11), channel_id=1, source_target_pairs={{0,2},{2,4},{4,6},{6,8},{8,10},{10,12},{12,14},{14,16},{16,18},{18... | collective-permute-start | bytes 1544 | tf_op jit(solution)/shard_map/ppermute | solution.py:21
  19.8 8.7 %collective-permute-start.3 = (s32[128]{0:T(128)S(1)}, s32[128]{0:T(128)S(1)}, u32[]{:S(2)}, u32[]{:S(2)}) collective-permute-start(s32[128]{0:T(128)S(1)} %get-tuple-element.12), channel_id=1, source_target_pairs={{2,0},{4,2},{6,4},{8,6},{10,8},{12,10},{14,12},{16,14},{18,16},{20... | collective-permute-start | bytes 1544 | tf_op jit(solution)/shard_map/ppermute | solution.py:22
  22.2 11.4 %collective-permute-start = (bf16[128,128]{0,1:T(8,128)(2,1)S(1)}, bf16[128,128]{0,1:T(8,128)(2,1)S(1)}, u32[]{:S(2)}, u32[]{:S(2)}) collective-permute-start(bf16[128,128]{0,1:T(8,128)(2,1)S(1)} %get-tuple-element.9), channel_id=1, source_target_pairs={{0,2},{2,4},{4,6},{6,8},{8,10},{10,12},{12,14},{14,16},{16,18},{18... | collective-permute-start | bytes 98312 | tf_op jit(solution)/shard_map/ppermute | solution.py:21
  27.2 6.7 %collective-permute-start.1 = (bf16[128,128]{0,1:T(8,128)(2,1)S(1)}, bf16[128,128]{0,1:T(8,128)(2,1)S(1)}, u32[]{:S(2)}, u32[]{:S(2)}) collective-permute-start(bf16[128,128]{0,1:T(8,128)(2,1)S(1)} %get-tuple-element.10), channel_id=1, source_target_pairs={{2,0},{4,2},{6,4},{8,6},{10,8},{12,10},{14,12},{16,14},{18,16},{20... | collective-permute-start | bytes 98312 | tf_op jit(solution)/shard_map/ppermute | solution.py:22
  37.6 149.7 %copy-start.2 = (f32[2048]{0:T(1024)S(1)}, f32[2048]{0:T(1024)}, u32[]{:S(2)}) copy-start(f32[2048]{0:T(1024)} %param.18) | copy-start | bytes 24580
  37.6 149.7 %all-gather.4.cloned.1.call-start = ((), (), s32[]{:S(2)}) async-start(), calls=%async_computation.1 | async-start | bytes 12255232 | tf_op jit(solution)/shard_map/all_gather | solution.py:91
  38.2 291.1 %all-gather.6.cloned.1.call-start = ((), (), s32[]{:S(2)}) async-start(), calls=%async_computation.2 | async-start | bytes 12255232 | tf_op jit(solution)/shard_map/all_gather | solution.py:92
  38.8 473.2 %all-gather.8.cloned.1.call-start = ((), (), s32[]{:S(2)}) async-start(), calls=%async_computation.3 | async-start | bytes 12255232 | tf_op jit(solution)/shard_map/all_gather | solution.py:96
  39.3 511.1 %all-reduce.5.cloned.1.call-start = ((), (), s32[]{:S(2)}) async-start(), calls=%async_computation.4 | async-start | bytes 3145728 | tf_op jit(solution)/shard_map/psum | solution.py:99
Sparse Core Ops, SparseCore 0:
  37.7 25.5 all-reduce.2
  531.9 18.5 all-reduce.4
Sparse Core Ops, SparseCore 1:
  40.8 146.4 all-gather.3
  189.9 139.3 all-gather.5
  331.8 180.0 all-gather.7
where the time goes:
time: 562 us
  waiting for transfers between devices  478 us (85%)
  matrix products  36.8 us (7%)
  starting transfers between devices  18.6 us (3%)
  between operations  15.2 us (3%)
  other arithmetic  10.5 us (2%)
    all_gather x1, waiting for transfers between devices, per_device(): lax.all_gather(down_weight, 'sp', axis=1, tiled=True)  183 us
    all_gather x1, waiting for transfers between devices, per_device(): up_acc = add_rows(lax.all_gather(up_weight, 'sp', axis=0, tiled=True))  130 us
    all_gather x1, waiting for transfers between devices, per_device(): gate_acc = add_rows(lax.all_gather(gate_weight, 'sp', axis=0, tiled=True))  120 us
    psum x1, waiting for transfers between devices, per_device(): branch = lax.psum(partial_value.astype(jnp.bfloat16), 'tp')  23.8 us
    dot_general x1, matrix products, per_device(): jnp.dot(hidden, lax.all_gather(down_weight, 'sp', axis=1, tiled=True), pr...  19.8 us
    psum x1, waiting for transfers between devices, per_device(): feed = lax.psum(terms.astype(jnp.bfloat16), 'tp')  18.7 us
    ppermute x3, starting transfers between devices, extended(): before = lax.ppermute(last, axis, up)  14.3 us
    dot_general x1, matrix products, add_rows(): return jnp.dot(normed, weight_rows, preferred_element_type=jnp.float32)  11.5 us
  transfers between devices with their start and end apart: 11, of which 6 were waited for; matrix products, arithmetic and copies ran while one was open for 4% of the time, Pallas kernels for 0%

commit v1 on v0

--- a/solution.py
+++ b/solution.py
@@ -93,7 +93,7 @@
     hidden = (jax.nn.silu(gate_acc) * up_acc).astype(jnp.bfloat16)
     terms = jnp.dot(
         hidden,
-        lax.all_gather(down_weight, "sp", axis=1, tiled=True),
+        jnp.concatenate(lax.all_gather(down_weight, "sp"), axis=1),
         preferred_element_type=jnp.float32,
     )
     feed = lax.psum(terms.astype(jnp.bfloat16), "tp")

time: 562 us -> 524 us (0.932)
  waiting for transfers between devices: 478 us -> 425 us
  local copies, waits for them, and re-layouts: 2.81 us -> 18 us
    all_gather x1, waiting for transfers between devices: 183 us -> 121 us  [per_device(): lax.all_gather(down_weight, 'sp')]
    reshape x0 -> x1, local copies, waits for them, and re-layouts: none -> 15.2 us  [per_device(): jnp.concatenate(lax.all_gather(down_weight, 'sp'), axis=1)]
    all_gather x1, waiting for transfers between devices: 120 us -> 127 us  [per_device(): gate_acc = add_rows(lax.all_gather(gate_weight, 'sp', axis=0, tiled=True))]
  transfers between devices with their start and end apart: 11 -> 11, of which waited for: 6 -> 6; matrix products, arithmetic and copies ran while one was open for 4% -> 7% of each run, Pallas kernels for 0% -> 0%
where the time goes in v1:
time: 524 us; the launch traced here: 523 us
  waiting for transfers between devices  425 us (81%)
  matrix products  37 us (7%)
  starting transfers between devices  18.6 us (4%)
  local copies, waits for them, and re-layouts  18 us (3%)
  between operations  15.2 us (3%)
  other arithmetic  9.58 us (2%)
    all_gather x1, waiting for transfers between devices, per_device(): up_acc = add_rows(lax.all_gather(up_weight, 'sp', axis=0, tiled=True))  132 us
    all_gather x1, waiting for transfers between devices, per_device(): gate_acc = add_rows(lax.all_gather(gate_weight, 'sp', axis=0, tiled=True))  127 us
    all_gather x1, waiting for transfers between devices, per_device(): lax.all_gather(down_weight, 'sp')  121 us
    psum x1, waiting for transfers between devices, per_device(): branch = lax.psum(partial_value.astype(jnp.bfloat16), 'tp')  23.8 us
    dot_general x1, matrix products, per_device(): jnp.dot(hidden, jnp.concatenate(lax.all_gather(down_weight, 'sp'), axis=1...  21.9 us
    psum x1, waiting for transfers between devices, per_device(): feed = lax.psum(terms.astype(jnp.bfloat16), 'tp')  18.7 us
    reshape x1, local copies, waits for them, and re-layouts, per_device(): jnp.concatenate(lax.all_gather(down_weight, 'sp'), axis=1)  15.2 us
    ppermute x3, starting transfers between devices, extended(): before = lax.ppermute(last, axis, up)  14.3 us
  transfers between devices with their start and end apart: 11, of which 6 were waited for; matrix products, arithmetic and copies ran while one was open for 7% of the time, Pallas kernels for 0%

profile of v1, /device:TPU:0, one launch (start us, length us, event | category | flops | bytes accessed | tf_op | source)
XLA Modules:
  0.0 523.2 jit_solution(14674159017082361998)
XLA Ops:
  7.4 0.9 fusion.38
  8.3 4.9 collective-permute-start.4
  13.2 1.3 collective-permute-start.5
  14.5 0.8 fusion.40
  15.2 4.5 collective-permute-start.2
  19.8 1.3 collective-permute-start.3
  21.1 1.0 constant_dynamic-slice_fusion.1
  22.2 4.9 collective-permute-start
  27.2 1.3 collective-permute-start.1
  29.2 1.4 fusion.14
  30.6 1.8 fusion.1
  32.5 1.0 fusion.6
  33.9 1.5 fusion.9
  35.4 2.2 convolution_convert_fusion.1
  39.6 23.8 %all-reduce.3.cloned.1.call-done = bf16[384,2048]{1,0:T(8,128)(2,1)} async-done(((bf16[384,2048]{1,0:T(8,128)(2,1)}), bf16[384,2048]{1,0:T(8,128)(2,1)}) %all-reduce.3.cloned.1.call-update) | async-done | bytes 1572880 | tf_op jit(solution)/shard_map/psum | solution.py:79
  63.3 2.6 fusion.2
  66.0 121.3 %all-gather.9.cloned.1.call-done = bf16[45056,128]{1,0:T(8,128)(2,1)} async-done(((bf16[2816,128]{1,0:T(8,128)(2,1)}), bf16[45056,128]{1,0:T(8,128)(2,1)}) %all-gather.9.cloned.1.call-update) | async-done | bytes 11534352 | tf_op jit(solution)/shard_map/all_gather | solution.py:96
  187.2 15.2 %copy.21 = bf16[2816,16,128]{0,2,1:T(8,128)(2,1)} copy(bf16[2816,16,128]{2,0,1:T(8,128)(2,1)} %bitcast.53) | data formatting | bytes 23068672 | tf_op jit(solution)/shard_map/reshape | solution.py:96
  202.5 126.8 %all-gather.5.cloned.1.call-done = bf16[2048,2816]{1,0:T(8,128)(2,1)} async-done(((bf16[128,2816]{1,0:T(8,128)(2,1)}), bf16[2048,2816]{1,0:T(8,128)(2,1)}) %all-gather.5.cloned.1.call-update) | async-done | bytes 11534352 | tf_op jit(solution)/shard_map/all_gather | solution.py:91
  329.3 9.7 %fusion.17 = f32[384,2816]{1,0:T(8,128)} fusion(bf16[2048,2816]{1,0:T(8,128)(2,1)} %all-gather.5.cloned.1.call-done, bf16[384,2048]{1,0:T(8,128)(2,1)S(1)} %get-tuple-element.6, f32[2048]{0:T(1024)S(1)} %copy-done.4, f32[384]{0:T(512)S(1)} %add_rsqrt_fusion), kind=kOutput, calls=%fused_computation.24 | convolution fusion | flops 4432330752 | bytes 17442304 | tf_op jit(solution)/shard_map/dot_general | solution.py:89
  338.9 132.3 %all-gather.7.cloned.1.call-done = bf16[2048,2816]{1,0:T(8,128)(2,1)} async-done(((bf16[128,2816]{1,0:T(8,128)(2,1)}), bf16[2048,2816]{1,0:T(8,128)(2,1)}) %all-gather.7.cloned.1.call-update) | async-done | bytes 11534352 | tf_op jit(solution)/shard_map/all_gather | solution.py:92
  471.3 21.9 %convolution_convert_fusion = bf16[384,2048]{1,0:T(8,128)(2,1)} fusion(bf16[2816,2048]{0,1:T(8,128)(2,1)} %bitcast.54, bf16[2048,2816]{1,0:T(8,128)(2,1)} %all-gather.7.cloned.1.call-done, f32[384,2816]{1,0:T(8,128)} %fusion.17, bf16[384,2048]{1,0:T(8,128)(2,1)} %copy-done.2, f32[2048]{0:T(1024)S(1)} %copy-done.4, f32[384]{0:T(512)S(1)} %add_rsqrt_fusion), kind=kOutput, calls=%fused_computation.14 | convolution fusion | flops 8868790272 | bytes 30549504 | tf_op jit(solution)/shard_map/dot_general | solution.py:94
  493.2 18.7 %all-reduce.5.cloned.1.call-done = bf16[384,2048]{1,0:T(8,128)(2,1)} async-done(((bf16[384,2048]{1,0:T(8,128)(2,1)}), bf16[384,2048]{1,0:T(8,128)(2,1)}) %all-reduce.5.cloned.1.call-update) | async-done | bytes 1572880 | tf_op jit(solution)/shard_map/psum | solution.py:99
  511.9 3.7 fusion.5
  (35 shorter events, 3.3 us)
Async XLA Ops:
  7.4 28.0 %copy-start = (bf16[512,2048]{1,0:T(8,128)(2,1)S(1)}, bf16[512,2048]{1,0:T(8,128)(2,1)}, u32[]{:S(2)}) copy-start(bf16[512,2048]{1,0:T(8,128)(2,1)} %param.17) | copy-start | bytes 6291460
  7.4 25.1 %copy-start.3 = (f32[4]{0:T(128)S(1)}, f32[4]{0:T(128)}, u32[]{:S(2)}) copy-start(f32[4]{0:T(128)} %param.16) | copy-start | bytes 52
  7.4 55.9 %all-reduce.3.cloned.1.call-start = ((), (), s32[]{:S(2)}) async-start(), calls=%async_computation | async-start | bytes 3145728 | tf_op jit(solution)/shard_map/psum | solution.py:79
  8.3 22.3 %collective-permute-start.4 = (bf16[128,128]{1,0:T(8,128)(2,1)S(1)}, bf16[128,128]{1,0:T(8,128)(2,1)S(1)}, u32[]{:S(2)}, u32[]{:S(2)}) collective-permute-start(bf16[128,128]{1,0:T(8,128)(2,1)S(1)} %get-tuple-element.7), channel_id=1, source_target_pairs={{0,2},{2,4},{4,6},{6,8},{8,10},{10,12},{12,14},{14,16},{16,18},{18... | collective-permute-start | bytes 98312 | tf_op jit(solution)/shard_map/ppermute | solution.py:21
  13.2 17.4 %collective-permute-start.5 = (bf16[128,128]{1,0:T(8,128)(2,1)S(1)}, bf16[128,128]{1,0:T(8,128)(2,1)S(1)}, u32[]{:S(2)}, u32[]{:S(2)}) collective-permute-start(bf16[128,128]{1,0:T(8,128)(2,1)S(1)} %get-tuple-element.8), channel_id=1, source_target_pairs={{2,0},{4,2},{6,4},{8,6},{10,8},{12,10},{14,12},{16,14},{18,16},{20... | collective-permute-start | bytes 98312 | tf_op jit(solution)/shard_map/ppermute | solution.py:22
  15.2 11.9 %collective-permute-start.2 = (s32[128]{0:T(128)S(1)}, s32[128]{0:T(128)S(1)}, u32[]{:S(2)}, u32[]{:S(2)}) collective-permute-start(s32[128]{0:T(128)S(1)} %get-tuple-element.11), channel_id=1, source_target_pairs={{0,2},{2,4},{4,6},{6,8},{8,10},{10,12},{12,14},{14,16},{16,18},{18... | collective-permute-start | bytes 1544 | tf_op jit(solution)/shard_map/ppermute | solution.py:21
  19.8 8.7 %collective-permute-start.3 = (s32[128]{0:T(128)S(1)}, s32[128]{0:T(128)S(1)}, u32[]{:S(2)}, u32[]{:S(2)}) collective-permute-start(s32[128]{0:T(128)S(1)} %get-tuple-element.12), channel_id=1, source_target_pairs={{2,0},{4,2},{6,4},{8,6},{10,8},{12,10},{14,12},{16,14},{18,16},{20... | collective-permute-start | bytes 1544 | tf_op jit(solution)/shard_map/ppermute | solution.py:22
  22.2 11.4 %collective-permute-start = (bf16[128,128]{0,1:T(8,128)(2,1)S(1)}, bf16[128,128]{0,1:T(8,128)(2,1)S(1)}, u32[]{:S(2)}, u32[]{:S(2)}) collective-permute-start(bf16[128,128]{0,1:T(8,128)(2,1)S(1)} %get-tuple-element.9), channel_id=1, source_target_pairs={{0,2},{2,4},{4,6},{6,8},{8,10},{10,12},{12,14},{14,16},{16,18},{18... | collective-permute-start | bytes 98312 | tf_op jit(solution)/shard_map/ppermute | solution.py:21
  27.2 6.7 %collective-permute-start.1 = (bf16[128,128]{0,1:T(8,128)(2,1)S(1)}, bf16[128,128]{0,1:T(8,128)(2,1)S(1)}, u32[]{:S(2)}, u32[]{:S(2)}) collective-permute-start(bf16[128,128]{0,1:T(8,128)(2,1)S(1)} %get-tuple-element.10), channel_id=1, source_target_pairs={{2,0},{4,2},{6,4},{8,6},{10,8},{12,10},{14,12},{16,14},{18,16},{20... | collective-permute-start | bytes 98312 | tf_op jit(solution)/shard_map/ppermute | solution.py:22
  37.6 149.7 %all-gather.9.cloned.1.call-start = ((), (), s32[]{:S(2)}) async-start(), calls=%async_computation.4 | async-start | bytes 12255232 | tf_op jit(solution)/shard_map/all_gather | solution.py:96
  38.2 291.1 %all-gather.5.cloned.1.call-start = ((), (), s32[]{:S(2)}) async-start(), calls=%async_computation.1 | async-start | bytes 12255232 | tf_op jit(solution)/shard_map/all_gather | solution.py:91
  38.7 432.5 %all-gather.7.cloned.1.call-start = ((), (), s32[]{:S(2)}) async-start(), calls=%async_computation.2 | async-start | bytes 12255232 | tf_op jit(solution)/shard_map/all_gather | solution.py:92
  39.3 472.6 %all-reduce.5.cloned.1.call-start = ((), (), s32[]{:S(2)}) async-start(), calls=%async_computation.3 | async-start | bytes 3145728 | tf_op jit(solution)/shard_map/psum | solution.py:99
  66.0 263.3 %copy-start.2 = (bf16[384,2048]{1,0:T(8,128)(2,1)}, bf16[384,2048]{1,0:T(8,128)(2,1)S(1)}, u32[]{:S(2)}) copy-start(bf16[384,2048]{1,0:T(8,128)(2,1)S(1)} %get-tuple-element.6) | copy-start | bytes 4718596
  187.2 142.0 %copy-start.4 = (f32[2048]{0:T(1024)S(1)}, f32[2048]{0:T(1024)}, u32[]{:S(2)}) copy-start(f32[2048]{0:T(1024)} %param.18) | copy-start | bytes 24580
  471.3 44.3 %copy-start.1 = (bf16[512,2048]{1,0:T(8,128)(2,1)S(1)}, bf16[512,2048]{1,0:T(8,128)(2,1)}, u32[]{:S(2)}) copy-start(bf16[512,2048]{1,0:T(8,128)(2,1)} %param.17) | copy-start | bytes 6291460
Sparse Core Ops, SparseCore 0:
  37.7 25.5 all-reduce.2
  493.3 18.5 all-reduce.4
Sparse Core Ops, SparseCore 1:
  40.8 146.4 all-gather.8
  189.9 139.3 all-gather.4
  331.9 139.3 all-gather.6
